TPU v7x, 128 devices: a whole 4x4x4 slice. The times are simulated.
128 devices in a mesh: sp: 16 (over z, x), tp: 8 (over y, core).
Axes of the slice: x: 4, y: 4, z: 4, core: 2. Of those that a mesh axis runs over, the one named last changes fastest.
Arguments:
- target: bfloat16 [8192, 4096], P(('sp', 'tp')), may hold values from -0.07 to 0.07
- source: bfloat16 [16384, 4096], P(('sp', 'tp')), may hold values from -0.035 to 0.035
- gain_target: float32 [4096], replicated, may hold values from 0.1 to 1.9
- gain_source: float32 [4096], replicated, may hold values from 0.1 to 1.9
- w_query: bfloat16 [4096, 1024], P(None, 'tp'), may hold values from -1 to 1
- w_key: bfloat16 [4096, 512], replicated, may hold values from -1 to 1
- w_value: bfloat16 [4096, 512], replicated, may hold values from -0.09375 to 0.09375
- w_out: bfloat16 [1024, 4096], P('tp'), may hold values from -0.1875 to 0.1875
- grad_output: bfloat16 [8192, 4096], P(('sp', 'tp')), may hold values from -6 to 6
Outputs:
- grad_target: float32 [8192, 4096], P(('sp', 'tp'))
- grad_source: float32 [16384, 4096], P(('sp', 'tp'))
- grad_out_proj: float32 [1024, 4096], P('tp')
All inputs are finite; a program needn't handle non-finite values.
Results may differ from a plain program's by a relative error of at most 0.028.
Values may be sent and summed in bfloat16 or wider, within the bound.
No kernel may reach another device: no remote copies, remote signals or barrier semaphores. Data moves between devices by JAX's collectives and lax.ppermute only.
A program may use at most 128 MiB of HBM per device.

v0:
```python
import math

import jax
import jax.numpy as jnp
from jax import lax
from jax.sharding import PartitionSpec as P

HD = 64


EPS = 1e-06


def sent_together(arrays, axis, dim, along):
    both = jnp.concatenate(arrays, axis=along)
    whole, at, finished = (lax.all_gather(both, axis, axis=dim, tiled=True), 0, [])
    for a in arrays:
        finished.append(lax.slice_in_dim(whole, at, at + a.shape[along], axis=along))
        at += a.shape[along]
    return tuple(finished)


def normalize(matrix, scaling):
    widened = matrix.astype(jnp.float32)
    factor = lax.rsqrt(jnp.mean(widened * widened, axis=-1, keepdims=True) + EPS)
    return (widened * factor * scaling).astype(jnp.bfloat16)


def norm_back(matrix, scaling, upstream):
    widened = matrix.astype(jnp.float32)
    factor = lax.rsqrt(jnp.mean(widened * widened, axis=-1, keepdims=True) + EPS)
    weighted = upstream * scaling
    inner = jnp.mean(widened * weighted, axis=-1, keepdims=True)
    return factor * weighted - widened * factor * factor * factor * inner


def score_block(queries, key_block, score_scale):
    return (
        jnp.einsum(
            "tkgd,skd->kgts", queries, key_block[:, :, 0], preferred_element_type=jnp.float32
        )
        * score_scale
    )


def split_arrived(arrived, key_count):
    row_count = arrived.shape[0]
    block_size = math.gcd(row_count, 1024)
    return (arrived.reshape(row_count // block_size, block_size, key_count, 2, HD), block_size)


def shards(target, source, gain_target, gain_source, w_query, w_key, w_value, w_out, grad_output):
    contract_last = (((1,), (1,)), ((), ()))
    across = lax.axis_size("tp")
    heads_all = w_key.shape[1] // HD
    key_count = heads_all // across
    query_count = w_query.shape[1] // HD
    group_size = query_count // key_count
    score_scale = float(HD) ** (-0.5)
    normed_target = normalize(target, gain_target)
    normed_source = normalize(source, gain_source)
    gathered_target, gathered_grad = sent_together((normed_target, grad_output), "tp", 0, 1)
    query = jnp.dot(gathered_target, w_query, preferred_element_type=jnp.float32).astype(
        jnp.bfloat16
    )
    head_grads = lax.dot_general(
        gathered_grad, w_out, contract_last, preferred_element_type=jnp.float32
    ).astype(jnp.bfloat16)
    row_count = query.shape[0]
    queries = query.reshape(row_count, key_count, group_size, HD)
    grad_heads = head_grads.reshape(row_count, key_count, group_size, HD)
    w_both = jnp.stack(
        [w_key.reshape(-1, heads_all, HD), w_value.reshape(-1, heads_all, HD)], axis=2
    )
    w_both = w_both.reshape(w_key.shape[0], heads_all * 2 * HD)
    pairs = jnp.dot(normed_source, w_both, preferred_element_type=jnp.float32).astype(jnp.bfloat16)
    own_pairs = lax.all_to_all(pairs, "tp", split_axis=1, concat_axis=0, tiled=True)
    start_max = jnp.full((key_count, group_size, row_count), -jnp.inf, jnp.float32)
    start_sum = jnp.zeros((key_count, group_size, row_count), jnp.float32)
    start_acc = jnp.zeros((row_count, key_count, group_size, HD), jnp.float32)
    blocks, block_size = split_arrived(
        lax.all_gather(own_pairs, "sp", axis=0, tiled=True), key_count
    )

    def absorb_advance(status, key_block):
        maxima, totals, accum = status
        scores = score_block(queries, key_block, score_scale)
        new_max = jnp.maximum(maxima, jnp.max(scores, axis=-1))
        shrink = jnp.exp(maxima - new_max)
        weights = jnp.exp(scores - new_max[..., None])
        totals = totals * shrink + jnp.sum(weights, axis=-1)
        partial_value = jnp.einsum(
            "kgts,skd->tkgd",
            weights.astype(jnp.bfloat16),
            key_block[:, :, 1],
            preferred_element_type=jnp.float32,
        )
        accum = accum * jnp.transpose(shrink, (2, 0, 1))[..., None] + partial_value
        return ((new_max, totals, accum), None)

    result, _ = lax.scan(absorb_advance, (start_max, start_sum, start_acc), blocks)
    maxima, totals, accum = result
    attn_heads = (accum / jnp.transpose(totals, (2, 0, 1))[..., None]).astype(jnp.bfloat16)
    delta_sum = jnp.sum(grad_heads.astype(jnp.float32) * attn_heads.astype(jnp.float32), axis=-1)
    delta_sum = jnp.transpose(delta_sum, (1, 2, 0))
    all_rows = own_pairs.shape[0] * lax.axis_size("sp")
    start_grad = jnp.zeros((row_count, key_count, group_size, HD), jnp.float32)
    start_pairs = jnp.zeros((all_rows, key_count * 2 * HD), jnp.float32)
    blocks, block_size = split_arrived(
        lax.all_gather(own_pairs, "sp", axis=0, tiled=True), key_count
    )

    def collect_advance(status, bundle):
        query_grad, pair_store = status
        key_block, position = bundle
        scores = score_block(queries, key_block, score_scale)
        attend = jnp.exp(scores - maxima[..., None]) / totals[..., None]
        grad_attend = jnp.einsum(
            "tkgd,skd->kgts", grad_heads, key_block[:, :, 1], preferred_element_type=jnp.float32
        )
        mixed = (attend * (grad_attend - delta_sum[..., None]) * score_scale).astype(jnp.bfloat16)
        query_grad = query_grad + jnp.einsum(
            "kgts,skd->tkgd", mixed, key_block[:, :, 0], preferred_element_type=jnp.float32
        )
        grad_key = jnp.einsum("kgts,tkgd->skd", mixed, queries, preferred_element_type=jnp.float32)
        grad_value = jnp.einsum(
            "kgts,tkgd->skd",
            attend.astype(jnp.bfloat16),
            grad_heads,
            preferred_element_type=jnp.float32,
        )
        stacked = jnp.stack([grad_key, grad_value], axis=2).reshape(block_size, key_count * 2 * HD)
        where_rows = position * block_size
        pair_store = lax.dynamic_update_slice_in_dim(pair_store, stacked, where_rows, 0)
        return ((query_grad, pair_store), None)

    positions = jnp.arange(blocks.shape[0], dtype=jnp.int32)
    result, _ = lax.scan(collect_advance, (start_grad, start_pairs), (blocks, positions))
    query_grad, pair_store = result
    pair_grads = lax.psum_scatter(
        pair_store.astype(jnp.bfloat16), "sp", scatter_dimension=0, tiled=True
    )
    grad_query = query_grad.astype(jnp.bfloat16).reshape(row_count, query_count * HD)
    pair_rows = lax.all_to_all(pair_grads, "tp", split_axis=0, concat_axis=1, tiled=True)
    grad_sn = lax.dot_general(pair_rows, w_both, contract_last, preferred_element_type=jnp.float32)
    grad_source = norm_back(source, gain_source, grad_sn)
    attention = attn_heads.reshape(row_count, query_count * HD)
    proj_part = lax.dot_general(
        attention, gathered_grad, (((0,), (0,)), ((), ())), preferred_element_type=jnp.float32
    )
    grad_out_proj = lax.psum(proj_part.astype(jnp.bfloat16), "sp").astype(jnp.float32)
    grad_xn = lax.psum_scatter(
        lax.dot_general(
            grad_query, w_query, contract_last, preferred_element_type=jnp.float32
        ).astype(jnp.bfloat16),
        "tp",
        scatter_dimension=0,
        tiled=True,
    ).astype(jnp.float32)
    grad_target = norm_back(target, gain_target, grad_xn)
    return (grad_target, grad_source, grad_out_proj)


def solution(mesh):
    return jax.shard_map(
        shards,
        mesh=mesh,
        in_specs=(
            P(("sp", "tp"), None),
            P(("sp", "tp"), None),
            P(),
            P(),
            P(None, "tp"),
            P(),
            P(),
            P("tp", None),
            P(("sp", "tp"), None),
        ),
        out_specs=(P(("sp", "tp"), None), P(("sp", "tp"), None), P("tp", None)),
        check_vma=False,
    )
```

profile of v0, /device:TPU:0, one launch (start us, length us, event | category | flops | bytes accessed | tf_op | source)
XLA Modules:
  0.0 473.2 jit_solution(16521432054210177134)
XLA Ops:
  8.8 6.5 %copy.31 = bf16[4096,512]{0,1:T(8,128)(2,1)} copy(bf16[4096,512]{1,0:T(8,128)(2,1)} %param.18) | data formatting | bytes 8388608 | tf_op args[5]
  15.3 6.4 %copy.32 = bf16[4096,512]{0,1:T(8,128)(2,1)} copy(bf16[4096,512]{1,0:T(8,128)(2,1)} %param.19) | data formatting | bytes 8388608 | tf_op args[6]
  21.7 7.4 %pad_maximum_fusion.1 = bf16[4096,8,2,64]{0,3,1,2:T(8,128)(2,1)} fusion(bf16[4096,8,1,64]{0,3,1,2:T(8,128)(2,1)} %bitcast.250, bf16[4096,8,1,64]{0,3,1,2:T(8,128)(2,1)} %bitcast.249), kind=kLoop, calls=%fused_computation.49 | loop fusion | flops 4194304 | bytes 16777216 | tf_op jit(solution)/shard_map/stack | solution.py:72
  29.1 7.8 %copy.33 = bf16[4096,8,2,64]{0,3,2,1:T(8,128)(2,1)} copy(bf16[4096,8,2,64]{0,3,1,2:T(8,128)(2,1)} %pad_maximum_fusion.1) | data formatting | bytes 16777216 | tf_op jit(solution)/shard_map/stack | solution.py:72
  37.0 6.4 %fusion.59 = bf16[16,8,8,128]{3,2,1,0:T(8,128)(2,1)S(1)} fusion(bf16[4096,1024]{0,1:T(8,128)(2,1)} %bitcast.246, bf16[128,4096]{1,0:T(8,128)(2,1)S(1)} %copy-done.1, f32[4096]{0:T(1024)S(1)} %copy-done.6, f32[128]{0:T(128)S(1)} %add_rsqrt_fusion), kind=kOutput, calls=%fused_computation.75 | convolution fusion | flops 1075970048 | bytes 9716224 | tf_op jit(solution)/shard_map/dot_general | solution.py:76
  43.4 12.0 %all_to_all.38 = bf16[128,8,128]{2,0,1:T(8,128)(2,1)} all-to-all(bf16[128,8,128]{2,0,1:T(8,128)(2,1)S(1)} %bitcast.259), channel_id=1, replica_groups=mesh['sp'=16,'tp'=8] {'tp'}, dimensions={1} | all-to-all | bytes 524288 | tf_op jit(solution)/shard_map/all_to_all | solution.py:77
  57.3 50.2 %all-gather.3.cloned.1.call-done = bf16[16384,128]{1,0:T(8,128)(2,1)} async-done(((bf16[1024,128]{1,0:T(8,128)(2,1)}), bf16[16384,128]{1,0:T(8,128)(2,1)}) %all-gather.3.cloned.1.call-update) | async-done | bytes 4194320 | tf_op jit(solution)/shard_map/all_gather | solution.py:110
  107.4 14.7 %reshape.168 = bf16[16,1024,1,2,64]{4,3,1,0,2:T(2,128)(2,1)} reshape(bf16[16384,128]{1,0:T(8,128)(2,1)} %all-gather.3.cloned.1.call-done) | data formatting | bytes 8388608 | tf_op jit(solution)/shard_map/reshape | solution.py:49
  122.1 20.3 %copy.37 = bf16[16,1024,1,2,64]{1,4,3,2,0:T(8,128)(2,1)} copy(bf16[16,1024,1,2,64]{4,3,1,0,2:T(2,128)(2,1)} %reshape.168) | data formatting | bytes 8388608
  142.4 16.5 %all-gather.5.cloned.1.call-done = bf16[512,8192]{1,0:T(8,128)(2,1)} async-done(((bf16[64,8192]{1,0:T(8,128)(2,1)}), bf16[512,8192]{1,0:T(8,128)(2,1)}) %all-gather.5.cloned.1.call-update) | async-done | bytes 8388624 | tf_op jit(solution)/shard_map/all_gather | solution.py:16
  159.0 3.7 fusion.63
  162.7 54.3 %while.28 = (s32[]{:T(128)}, f32[1,2,512]{2,1,0:T(2,128)S(1)}, f32[1,2,512]{2,1,0:T(2,128)S(1)}, f32[512,1,2,64]{0,3,2,1:T(8,128)S(1)}, bf16[16,1024,1,2,64]{1,4...) while((s32[]{:T(128)}, f32[1,2,512]{2,1,0:T(2,128)S(1)}, ...), condition=%wide.region_5.6_spmd.clone, body=%wide.region_2.5_spmd.clone.sunk | while | flops 277026816 | bytes 14090349 | solution.py:101
  217.0 4.0 fusion.60
  221.1 3.9 convolution_convert_fusion.1
  225.0 2.2 broadcast_in_dim.6.clone
  227.3 110.4 %while.29 = (s32[]{:T(128)}, f32[512,1,2,64]{0,3,2,1:T(8,128)S(1)}, bf16[16384,128]{1,0:T(8,128)(2,1)}, bf16[16,1024,1,2,64]{1,4,3,2,0:T(8,128)(2,1)}, bf16[512,...) while((s32[]{:T(128)}, f32[512,1,2,64]{0,3,2,1:T(8,128)S(1)}, ...), condition=%wide.region_8.9_spmd.clone, body=%wide.region_7.8_spmd.clone.sunk | while | flops 679739392 | bytes 22687960 | solution.py:138
  337.8 3.3 convolution_convert_fusion
  341.1 2.8 convert_element_type.82
  343.9 72.7 %reduce-scatter.5.cloned.1.call-done = bf16[1024,128]{1,0:T(8,128)(2,1)} async-done(((bf16[16384,128]{1,0:T(8,128)(2,1)}), bf16[1024,128]{1,0:T(8,128)(2,1)}) %reduce-scatter.5.cloned.1.call-update) | async-done | bytes 262160 | tf_op jit(solution)/shard_map/reduce_scatter | solution.py:140
  416.7 4.3 all-to-all-start.1
  421.0 35.0 %reduce-scatter.3.cloned.1.call-done = bf16[64,4096]{1,0:T(8,128)(2,1)} async-done(((bf16[512,4096]{1,0:T(8,128)(2,1)}), bf16[64,4096]{1,0:T(8,128)(2,1)}) %reduce-scatter.3.cloned.1.call-update) | async-done | bytes 524304 | tf_op jit(solution)/shard_map/reduce_scatter | solution.py:152
  457.3 2.4 fusion.69
  459.9 4.9 %fusion.56 = (f32[128]{0:T(128)S(1)}, f32[128,4096]{1,0:T(8,128)S(1)}) fusion(bf16[128,4096]{1,0:T(8,128)(2,1)S(1)} %copy-done.1, f32[4096]{0:T(1024)S(1)} %copy-done.6, bf16[128,1024]{0,1:T(8,128)(2,1)S(1)} %bitcast.256, bf16[4096,1024]{0,1:T(8,128)(2,1)} %bitcast.247), kind=kOutput, calls=%fused_computation.68 | convolution fusion | flops 1075838848 | bytes 11813376 | tf_op jit(solution)/shard_map/dot_general | solution.py:145
  464.8 1.9 fusion.54
  (316 shorter events, 158.0 us)
Async XLA Ops:
  7.2 151.8 %copy-start = (bf16[4096,128]{1,0:T(8,128)(2,1)S(1)}, bf16[4096,128]{1,0:T(8,128)(2,1)}, u32[]{:S(2)}) copy-start(bf16[4096,128]{1,0:T(8,128)(2,1)} %param.17) | copy-start | bytes 3145732
  7.2 100.2 %all-gather.3.cloned.1.call-start = ((), (), s32[]{:S(2)}) async-start(), calls=%async_computation.4 | async-start | bytes 4456448 | tf_op jit(solution)/shard_map/all_gather | solution.py:110
  29.1 7.8 %copy-start.1 = (bf16[128,4096]{1,0:T(8,128)(2,1)S(1)}, bf16[128,4096]{1,0:T(8,128)(2,1)}, u32[]{:S(2)}) copy-start(bf16[128,4096]{1,0:T(8,128)(2,1)} %param.14) | copy-start | bytes 3145732
  29.1 7.8 %copy-start.6 = (f32[4096]{0:T(1024)S(1)}, f32[4096]{0:T(1024)}, u32[]{:S(2)}) copy-start(f32[4096]{0:T(1024)} %param.16) | copy-start | bytes 49156
  36.9 18.5 %copy-start.2 = (bf16[64,4096]{1,0:T(8,128)(2,1)S(1)}, bf16[64,4096]{1,0:T(8,128)(2,1)}, u32[]{:S(2)}) copy-start(bf16[64,4096]{1,0:T(8,128)(2,1)} %param.13) | copy-start | bytes 1572868
  36.9 18.8 %copy-start.5 = (f32[4096]{0:T(1024)S(1)}, f32[4096]{0:T(1024)}, u32[]{:S(2)}) copy-start(f32[4096]{0:T(1024)} %param.15) | copy-start | bytes 49156
  36.9 19.0 %copy-start.4 = (bf16[64,4096]{1,0:T(8,128)(2,1)S(1)}, bf16[64,4096]{1,0:T(8,128)(2,1)}, u32[]{:S(2)}) copy-start(bf16[64,4096]{1,0:T(8,128)(2,1)} %param.21) | copy-start | bytes 1572868
  55.4 103.6 %all-gather.5.cloned.1.call-start = ((), (), s32[]{:S(2)}) async-start(), calls=%async_computation.5 | async-start | bytes 9437184 | tf_op jit(solution)/shard_map/all_gather | solution.py:16
  57.0 284.1 %all-reduce.2.cloned.1.call-start = ((), (), s32[]{:S(2)}) async-start(), calls=%async_computation.8 | async-start | bytes 2097152 | tf_op jit(solution)/shard_map/psum | solution.py:151
  225.0 191.7 %reduce-scatter.5.cloned.1.call-start = ((), (), s32[]{:S(2)}) async-start(), calls=%async_computation.7 | async-start | bytes 4456448 | tf_op jit(solution)/shard_map/reduce_scatter | solution.py:140
  337.7 118.2 %reduce-scatter.3.cloned.1.call-start = ((), (), s32[]{:S(2)}) async-start(), calls=%async_computation.6 | async-start | bytes 4718592 | tf_op jit(solution)/shard_map/reduce_scatter | solution.py:152
  341.1 114.9 %copy-start.3 = (bf16[64,4096]{1,0:T(8,128)(2,1)S(1)}, bf16[64,4096]{1,0:T(8,128)(2,1)}, u32[]{:S(2)}) copy-start(bf16[64,4096]{1,0:T(8,128)(2,1)} %param.13) | copy-start | bytes 1572868
  416.7 43.0 %all-to-all-start.1 = ((bf16[8,128,128]{2,1,0:T(8,128)(2,1)}), bf16[8,128,128]{2,1,0:T(8,128)(2,1)S(1)}, u32[]{:S(2)}, u32[]{:S(2)}) async-start(bf16[8,128,128]{2,1,0:T(8,128)(2,1)} %bitcast.262), calls=%async_computation.3 | async-start | bytes 524288 | tf_op jit(solution)/shard_map/all_to_all | solution.py:144
Sparse Core Ops, SparseCore 0:
  55.5 51.8 all-gather.2
  109.7 49.2 all-gather.4
  225.1 87.6 all-reduce.1
  337.9 78.7 reduce-scatter.4
  418.9 37.0 reduce-scatter.2
where the time goes:
time: 476 us; the launch traced here: 473 us
  waiting for transfers between devices  175 us (37%)
  local copies, waits for them, and re-layouts  113 us (24%)
  matrix products  112 us (24%)
  other arithmetic  31.2 us (7%)
  between operations  14 us (3%)
  blocking collectives  12 us (3%)
  loops' own time  12 us (3%)
    reduce_scatter x1, waiting for transfers between devices, shards(): lax.psum_scatter(pair_store.astype(jnp.bfloat16), 'sp', scatter_dimension...  72.7 us
    all_gather x1, waiting for transfers between devices, shards(): lax.all_gather(own_pairs, 'sp', axis=0, tiled=True)  50.2 us
    reduce_scatter x1, waiting for transfers between devices, shards(): lax.psum_scatter(lax.dot_general(grad_query, w_query, contract_last, pref...  35 us
    unnamed x17, local copies, waits for them, and re-layouts  33.2 us
    squeeze x32, local copies, waits for them, and re-layouts, shards(): lax.scan(absorb_advance, (start_max, start_sum, start_acc), blocks)  31.2 us
    dot_general x32, matrix products, score_block(): jnp.einsum('tkgd,skd->kgts', queries, key_block[:, :, 0], preferred_eleme...  27.3 us
    all_gather x1, waiting for transfers between devices, sent_together(): lax.all_gather(both, axis, axis=dim, tiled=True)  16.5 us
    reshape x1, local copies, waits for them, and re-layouts, split_arrived(): arrived.reshape(row_count // block_size, block_size, key_count, 2, HD)  14.7 us
  transfers between devices with their start and end apart: 6, of which 4 were waited for; matrix products, arithmetic and copies ran while one was open for 31% of the time, Pallas kernels for 0%

commit v1 on v0

v1 whole, which is shorter than its diff:
```python
import functools
import math

import jax
import jax.numpy as jnp
from jax import lax
from jax.experimental import pallas as pl
from jax.experimental.pallas import tpu as pltpu
from jax.sharding import Mesh
from jax.sharding import PartitionSpec as P

HD = 64
EPS = 1e-06
NZ = 4
NX = 4
BF = jnp.bfloat16
F32 = jnp.float32
NT = (((1,), (1,)), ((), ()))


def normalize(matrix, scaling):
    widened = matrix.astype(F32)
    factor = lax.rsqrt(jnp.mean(widened * widened, axis=-1, keepdims=True) + EPS)
    return (widened * factor * scaling).astype(BF)


def pairs_kernel(x_ref, g_ref, wk_ref, wv_ref, out_ref, sn):
    @pl.when(pl.program_id(0) == 0)
    def _():
        sn[...] = normalize(x_ref[...], g_ref[...])

    k = jnp.dot(sn[...], wk_ref[...], preferred_element_type=F32).astype(BF)
    v = jnp.dot(sn[...], wv_ref[...], preferred_element_type=F32).astype(BF)
    out_ref[0] = jnp.concatenate([k[:, :HD], v[:, :HD]], axis=1)
    out_ref[1] = jnp.concatenate([k[:, HD:], v[:, HD:]], axis=1)


def project_pairs(source, gain, w_key, w_value):
    rows, width = source.shape
    heads = w_key.shape[1] // HD
    return pl.pallas_call(
        pairs_kernel,
        grid=(heads // 2,),
        in_specs=[
            pl.BlockSpec((rows, width), lambda i: (0, 0)),
            pl.BlockSpec((1, width), lambda i: (0, 0)),
            pl.BlockSpec((width, 2 * HD), lambda i: (0, i)),
            pl.BlockSpec((width, 2 * HD), lambda i: (0, i)),
        ],
        out_specs=pl.BlockSpec((2, rows, 2 * HD), lambda i: (i, 0, 0)),
        out_shape=jax.ShapeDtypeStruct((heads, rows, 2 * HD), BF),
        scratch_shapes=[pltpu.VMEM((rows, width), BF)],
        name="pairs",
    )(source, gain.reshape(1, width), w_key, w_value)


def forward_kernel(qt_ref, kv_ref, o_ref, st_ref, e_ref, kvt_ref, vt1, sbuf, *, nj):
    first = (pl.program_id(0) == 0) & (pl.program_id(1) == 0)
    src = kv_ref.shape[1]

    @pl.when(first)
    def _():
        row = lax.broadcasted_iota(jnp.int32, (16, src), 0)
        ones = jnp.where(row == 0, 1.0, 0.0).astype(BF)
        for j in range(nj):
            turned = kv_ref[j].T
            kvt_ref[j] = turned
            vt1[j, 0:HD, :] = turned[HD:, :]
            vt1[j, HD:, :] = ones

    q = qt_ref[0]
    highest = None
    acc = None
    sbuf[0] = jnp.dot(kv_ref[0, :, 0:HD], q, preferred_element_type=F32)
    for j in range(nj):
        if j + 1 < nj:
            sbuf[(j + 1) % 2] = jnp.dot(kv_ref[j + 1, :, 0:HD], q, preferred_element_type=F32)
        s = sbuf[j % 2]
        top = jnp.max(s, axis=0, keepdims=True)
        new = top if highest is None else jnp.maximum(highest, top)
        e = jnp.exp2(s - new).astype(BF)
        e_ref[j, 0] = e
        part = jnp.dot(vt1[j], e, preferred_element_type=F32)
        acc = part if acc is None else acc * jnp.exp2(highest - new) + part
        highest = new
        st_ref[0, 0, j : j + 1, :] = new
    total = acc[HD : HD + 1]
    st_ref[0, 0, nj : nj + 1, :] = total
    o_ref[0] = (acc[0:HD] / total).astype(BF)


def forward(qt, kv):
    nk, width, tgt = qt.shape
    nj, src, _ = kv.shape
    nh = width // HD
    return pl.pallas_call(
        functools.partial(forward_kernel, nj=nj),
        grid=(nk, nh),
        in_specs=[
            pl.BlockSpec((1, HD, tgt), lambda k, h: (k, h, 0)),
            pl.BlockSpec((nj, src, 2 * HD), lambda k, h: (0, 0, 0)),
        ],
        out_specs=[
            pl.BlockSpec((1, HD, tgt), lambda k, h: (k, h, 0)),
            pl.BlockSpec((1, 1, 8, tgt), lambda k, h: (k, h, 0, 0)),
            pl.BlockSpec((nj, 1, src, tgt), lambda k, h: (0, k * nh + h, 0, 0)),
            pl.BlockSpec((nj, 2 * HD, src), lambda k, h: (0, 0, 0)),
        ],
        out_shape=[
            jax.ShapeDtypeStruct((nk, width, tgt), BF),
            jax.ShapeDtypeStruct((nk, nh, 8, tgt), F32),
            jax.ShapeDtypeStruct((nj, nk * nh, src, tgt), BF),
            jax.ShapeDtypeStruct((nj, 2 * HD, src), BF),
        ],
        scratch_shapes=[pltpu.VMEM((nj, HD + 16, src), BF), pltpu.VMEM((2, src, tgt), F32)],
        cost_estimate=pl.CostEstimate(
            flops=40_000_000_000, transcendentals=nj * nk * nh * src * tgt, bytes_accessed=40_000_000
        ),
        name="forward",
    )(qt, kv)


def backward_kernel(
    j0, w_ref, qt_ref, dot_ref, kv_ref, kvt_ref, e_ref, dq_in, dkv_ref, dq_ref, vaug, rhs, store
):
    j = pl.program_id(0)
    i = pl.program_id(1)
    src = kv_ref.shape[1]
    tgt = qt_ref.shape[2]

    @pl.when(i == 0)
    def _():
        lane = lax.broadcasted_iota(jnp.int32, (src, HD), 1)
        vaug[:, 0:HD] = kv_ref[0, :, HD:]
        vaug[:, HD:] = jnp.where(lane < 2, 1.0, 0.0).astype(BF)

    @pl.when((i == 0) & (j == 0))
    def _():
        rhs[...] = jnp.zeros_like(rhs)

    share = w_ref[0, 0, pl.ds(j + j0, 1), :]
    delta = w_ref[0, 0, 4:5, :] * share
    high = delta.astype(BF).astype(F32)
    low = delta - high
    dos = (dot_ref[0].astype(F32) * share).astype(BF)
    rhs[0:HD, :] = dos
    row = lax.broadcasted_iota(jnp.int32, (16, tgt), 0)
    rhs[HD : HD + 16, :] = jnp.where(row == 0, -high, jnp.where(row == 1, -low, 0.0)).astype(BF)
    dp = jnp.dot(vaug[...], rhs[...], preferred_element_type=F32)
    e = e_ref[0, 0]
    g = e * dp.astype(BF)
    dv = lax.dot_general(dos, e, NT, preferred_element_type=F32)
    dk = lax.dot_general(qt_ref[0], g, NT, preferred_element_type=F32)

    @pl.when(i == 0)
    def _():
        store[0:HD, :] = dk
        store[HD:, :] = dv

    @pl.when(i > 0)
    def _():
        store[0:HD, :] += dk
        store[HD:, :] += dv

    @pl.when(i == pl.num_programs(1) - 1)
    def _():
        row = lax.broadcasted_iota(jnp.int32, (2 * HD, 1), 0)
        scale = jnp.where(row < HD, math.log(2.0), 1.0)
        dkv_ref[0] = (store[...] * scale).T.astype(dkv_ref.dtype)

    dq = jnp.dot(kvt_ref[0, 0:HD, :], g, preferred_element_type=F32)

    @pl.when(j == 0)
    def _():
        dq_ref[i] = dq_in[i] + dq

    @pl.when(j > 0)
    def _():
        dq_ref[i] += dq


def backward(w, qt, dot, kv, kvt, e, dq_in, j0, njc, dtype):
    nk, width, tgt = qt.shape
    src = kv.shape[1]
    nh = width // HD
    nb = nk * nh
    return pl.pallas_call(
        functools.partial(backward_kernel, j0),
        grid=(njc, nb),
        in_specs=[
            pl.BlockSpec((1, 1, 8, tgt), lambda j, i: (i // nh, i % nh, 0, 0)),
            pl.BlockSpec((1, HD, tgt), lambda j, i: (i // nh, i % nh, 0)),
            pl.BlockSpec((1, HD, tgt), lambda j, i: (i // nh, i % nh, 0)),
            pl.BlockSpec((1, src, 2 * HD), lambda j, i: (j + j0, 0, 0)),
            pl.BlockSpec((1, 2 * HD, src), lambda j, i: (j + j0, 0, 0)),
            pl.BlockSpec((1, 1, src, tgt), lambda j, i: (j + j0, i, 0, 0)),
            pl.BlockSpec((nb, HD, tgt), lambda j, i: (0, 0, 0)),
        ],
        out_specs=[
            pl.BlockSpec((1, src, 2 * HD), lambda j, i: (j, 0, 0)),
            pl.BlockSpec((nb, HD, tgt), lambda j, i: (0, 0, 0)),
        ],
        out_shape=[
            jax.ShapeDtypeStruct((njc, src, 2 * HD), dtype),
            jax.ShapeDtypeStruct((nb, HD, tgt), F32),
        ],
        scratch_shapes=[
            pltpu.VMEM((src, 2 * HD), BF),
            pltpu.VMEM((2 * HD, tgt), BF),
            pltpu.VMEM((2 * HD, src), F32),
        ],
        cost_estimate=pl.CostEstimate(
            flops=17_000_000_000 * njc, transcendentals=0, bytes_accessed=9_000_000 * njc
        ),
        name="backward%d" % j0,
    )(w, qt, dot, kv, kvt, e, dq_in)


def norm_back(x, scaling, upstream):
    widened = x.astype(F32)
    factor = lax.rsqrt(jnp.mean(widened * widened, axis=-1, keepdims=True) + EPS)
    weighted = upstream * scaling
    inner = jnp.mean(widened * weighted, axis=-1, keepdims=True)
    return factor * weighted - widened * factor * factor * factor * inner


def source_kernel(dkv_ref, wk_ref, wv_ref, x_ref, g_ref, out_ref, dk, dv, dsn):
    i = pl.program_id(0)
    heads = dkv_ref.shape[0]
    cols = wk_ref.shape[0]

    @pl.when(i == 0)
    def _():
        for h in range(heads):
            dk[:, h * HD : (h + 1) * HD] = dkv_ref[h, :, :HD]
            dv[:, h * HD : (h + 1) * HD] = dkv_ref[h, :, HD:]

    part = lax.dot_general(dk[...], wk_ref[...], NT, preferred_element_type=F32)
    part = part + lax.dot_general(dv[...], wv_ref[...], NT, preferred_element_type=F32)
    dsn[:, pl.ds(pl.multiple_of(i * cols, cols), cols)] = part

    @pl.when(i == pl.num_programs(0) - 1)
    def _():
        out_ref[...] = norm_back(x_ref[...], g_ref[...], dsn[...])


def source_grad(dkv, w_key, w_value, source, gain):
    heads, rows, _ = dkv.shape
    width = source.shape[1]
    steps = 8
    cols = width // steps
    return pl.pallas_call(
        source_kernel,
        grid=(steps,),
        in_specs=[
            pl.BlockSpec((heads, rows, 2 * HD), lambda i: (0, 0, 0)),
            pl.BlockSpec((cols, heads * HD), lambda i: (i, 0)),
            pl.BlockSpec((cols, heads * HD), lambda i: (i, 0)),
            pl.BlockSpec((rows, width), lambda i: (0, 0)),
            pl.BlockSpec((1, width), lambda i: (0, 0)),
        ],
        out_specs=pl.BlockSpec((rows, width), lambda i: (0, 0)),
        out_shape=jax.ShapeDtypeStruct((rows, width), F32),
        scratch_shapes=[
            pltpu.VMEM((rows, heads * HD), BF),
            pltpu.VMEM((rows, heads * HD), BF),
            pltpu.VMEM((rows, width), F32),
        ],
        name="source_grad",
    )(dkv, w_key, w_value, source, gain.reshape(1, width))


def target_kernel(dq_ref, wq_ref, x_ref, g_ref, out_ref, dxn):
    i = pl.program_id(0)
    parts = dq_ref.shape[0]
    cols = wq_ref.shape[1]
    part = None
    for t in range(parts):
        one = lax.dot_general(dq_ref[t], wq_ref[t], NT, preferred_element_type=F32)
        part = one if part is None else part + one
    dxn[:, pl.ds(pl.multiple_of(i * cols, cols), cols)] = part

    @pl.when(i == pl.num_programs(0) - 1)
    def _():
        out_ref[...] = norm_back(x_ref[...], g_ref[...], dxn[...])


def target_grad(dq, w_all, target, gain):
    parts, rows, part_width = dq.shape
    width = target.shape[1]
    steps = 8
    cols = width // steps
    return pl.pallas_call(
        target_kernel,
        grid=(steps,),
        in_specs=[
            pl.BlockSpec((parts, rows, part_width), lambda i: (0, 0, 0)),
            pl.BlockSpec((parts, cols, part_width), lambda i: (0, i, 0)),
            pl.BlockSpec((rows, width), lambda i: (0, 0)),
            pl.BlockSpec((1, width), lambda i: (0, 0)),
        ],
        out_specs=pl.BlockSpec((rows, width), lambda i: (0, 0)),
        out_shape=jax.ShapeDtypeStruct((rows, width), F32),
        scratch_shapes=[pltpu.VMEM((rows, width), F32)],
        name="target_grad",
    )(dq, w_all, target, gain.reshape(1, width))


def take_from(a, axis, size, shift):
    return lax.ppermute(a, axis, [((i + shift) % size, i) for i in range(size)])


def give_to(a, axis, size, shift):
    return lax.ppermute(a, axis, [(i, (i + shift) % size) for i in range(size)])


def gathered(a, axis, size):
    return jnp.stack([a] + [take_from(a, axis, size, k) for k in range(1, size)])


def turned(a, shift):
    return a if shift == 0 else jnp.concatenate([a[-shift:], a[:-shift]])


def shards(target, source, gain_target, gain_source, w_query, w_key, w_value, w_out, grad_output):
    across = lax.axis_size("tp")
    local = target.shape[0]
    width = target.shape[1]

    normed_target = normalize(target, gain_target)
    all_target = lax.all_gather(normed_target, "tp", axis=0, tiled=True)
    pairs = project_pairs(source, gain_source, w_key, w_value)
    own_pairs = lax.all_to_all(pairs, "tp", split_axis=0, concat_axis=0, tiled=True)
    kv = gathered(own_pairs.reshape(-1, 2 * HD), "x", NX)

    score_scale = math.log2(math.e) / math.sqrt(HD)
    own_qt = lax.dot_general(
        w_query, all_target, (((0,), (1,)), ((), ())), preferred_element_type=F32
    )
    own_qt = (own_qt * score_scale).astype(BF)
    qt = gathered(own_qt, "z", NZ)

    grad_output, _ = lax.optimization_barrier((grad_output, all_target))
    all_grad = lax.all_gather(grad_output, "tp", axis=0, tiled=True)
    own_dot = lax.dot_general(w_out, all_grad, NT, preferred_element_type=F32).astype(BF)
    dot = gathered(own_dot, "z", NZ)

    w_first, _ = lax.optimization_barrier((w_query, all_grad))
    w_all = lax.all_gather(w_first, "tp", axis=0, tiled=False)

    o_part, stats, e, kvt = forward(qt, kv)
    nk, wide, tgt = qt.shape
    nh = wide // HD

    def by_head(a):
        return a.astype(F32).reshape(nk, nh, HD, tgt)

    delta_part = jnp.sum(by_head(dot) * by_head(o_part), axis=2)
    top_part, sum_part = stats[:, :, NX - 1], stats[:, :, NX]
    small = jnp.stack([top_part, sum_part, delta_part], axis=1)
    smalls = [small] + [turned(take_from(small, "z", NZ, s), s) for s in range(1, NZ)]
    top = functools.reduce(jnp.maximum, [s[:, 0] for s in smalls])
    shares = [jnp.exp2(s[:, 0] - top) * s[:, 1] for s in smalls]
    total = sum(shares)
    delta = sum(w * s[:, 2] for w, s in zip(shares, smalls)) / total
    chunk_share = jnp.exp2(stats[:, :, 0:NX] - top[:, :, None]) / total[:, :, None]
    weights = jnp.concatenate(
        [chunk_share, delta[:, :, None], jnp.zeros((nk, nh, 3, tgt), F32)], axis=2
    )

    o = 0.0
    for k in range(NZ):
        got = o_part[0] if k == 0 else give_to(o_part[k], "z", NZ, k)
        part_share = shares[(NZ - k) % NZ][0] / total[0]
        o = o + got.astype(F32).reshape(nh, HD, tgt) * part_share[:, None]
    o = o.astype(BF).reshape(wide, tgt)
    proj_part = lax.dot_general(
        o, all_grad, (((1,), (0,)), ((), ())), preferred_element_type=F32
    ).astype(BF)
    grad_out_proj = lax.psum(proj_part, ("z", "x")).astype(F32)

    dq_zero = jnp.zeros((nk * nh, HD, tgt), F32)
    dkv_far, dq_far = backward(weights, qt, dot, kv, kvt, e, dq_zero, 1, NX - 1, BF)
    dkv_got = [give_to(dkv_far[j - 1], "x", NX, j) for j in range(1, NX)]
    dkv_own, dq_all = backward(weights, qt, dot, kv, kvt, e, dq_far, 0, 1, F32)

    dq_all = (dq_all * (1.0 / math.sqrt(HD))).reshape(nk, wide, tgt)
    dq_got = [give_to(dq_all[k].astype(BF), "z", NZ, k) for k in range(1, NZ)]

    dkv = dkv_own[0] + sum(d.astype(F32) for d in dkv_got)
    dkv = dkv.astype(BF).reshape(across, -1, 2 * HD)
    dkv = lax.all_to_all(dkv, "tp", split_axis=0, concat_axis=0, tiled=True)
    grad_source = source_grad(dkv, w_key, w_value, source, gain_source)

    dq = dq_all[0] + sum(d.astype(F32) for d in dq_got)
    dq = dq.T.astype(BF).reshape(across, local, wide)
    dq = lax.all_to_all(dq, "tp", split_axis=0, concat_axis=0, tiled=True)
    grad_target = target_grad(dq, w_all, target, gain_target)
    return (grad_target, grad_source, grad_out_proj)


def solution(mesh):
    fine = Mesh(mesh.devices.reshape(NZ, NX, -1), ("z", "x", "tp"))
    rows = P(("z", "x", "tp"), None)
    return jax.shard_map(
        shards,
        mesh=fine,
        in_specs=(rows, rows, P(), P(), P(None, "tp"), P(), P(), P("tp", None), rows),
        out_specs=(rows, rows, P("tp", None)),
        check_vma=False,
    )
```

time: 476 us -> 297 us (0.62)
  Pallas kernels: 0 us -> 111 us
  local copies, waits for them, and re-layouts: 113 us -> 4.1 us
  matrix products: 112 us -> 9.34 us
  waiting for transfers between devices: 175 us -> 91 us
  starting transfers between devices: 4.68 us -> 38.4 us
  other arithmetic: 31.2 us -> 13.5 us
  loops' own time: 12 us -> 0 us
    pallas_call x0 -> x6, Pallas kernels: none -> 111 us  [the longest x2 53.9 us: backward(): pl.pallas_call(functools.partial(backward_kernel, j0), grid=(njc, nb), in...]
    reduce_scatter x2 -> x0, waiting for transfers between devices: 108 us -> none  [the longest x1 72.7 us: shards(): lax.psum_scatter(pair_store.astype(jnp.bfloat16), 'sp', scatter_dimension...]
    dot_general x118 -> x3, matrix products: 112 us -> 9.34 us  [the longest x1 3.87 us: shards(): lax.dot_general(w_out, all_grad, NT, preferred_element_type=F32).astype(BF)]
    unnamed x17 -> x20, local copies, waits for them, and re-layouts: 33.2 us -> 0.07 us
    ppermute x0 -> x21, starting transfers between devices: none -> 31.4 us  [the longest x12 21.5 us: take_from(): return lax.ppermute(a, axis, [((i + shift) % size, i) for i in range(size)])]
    squeeze x32 -> x3, local copies, waits for them, and re-layouts: 31.2 us -> 1.32 us  [the longest x1 1.16 us: shards(): dkv_got = [give_to(dkv_far[j - 1], 'x', NX, j) for j in range(1, NX)]]
    reshape x1 -> x0, local copies, waits for them, and re-layouts: 14.7 us -> none  [split_arrived(): arrived.reshape(row_count // block_size, block_size, key_count, 2, HD)]
    dynamic_update_slice x32 -> x0, local copies, waits for them, and re-layouts: 14.4 us -> none  [collect_advance(): lax.dynamic_update_slice_in_dim(pair_store, stacked, where_rows, 0)]
  transfers between devices with their start and end apart: 6 -> 27, of which waited for: 4 -> 12; matrix products, arithmetic and copies ran while one was open for 31% -> 6% of each run, Pallas kernels for 0% -> 34%
where the time goes in v1:
time: 297 us; the launch traced here: 295 us
  Pallas kernels  111 us (37%)
  waiting for transfers between devices  91 us (31%)
  starting transfers between devices  38.4 us (13%)
  between operations  14.1 us (5%)
  blocking collectives  13.8 us (5%)
  other arithmetic  13.5 us (5%)
  matrix products  9.34 us (3%)
  local copies, waits for them, and re-layouts  4.1 us (1%)
    pallas_call x2, Pallas kernels, backward(): pl.pallas_call(functools.partial(backward_kernel, j0), grid=(njc, nb), in...  53.9 us
    all_gather x1, waiting for transfers between devices, shards(): w_all = lax.all_gather(w_first, 'tp', axis=0, tiled=False)  38.7 us
    all_gather x1, waiting for transfers between devices, shards(): all_target = lax.all_gather(normed_target, 'tp', axis=0, tiled=True)  34.7 us
    pallas_call x1, Pallas kernels, forward(): pl.pallas_call(functools.partial(forward_kernel, nj=nj), grid=(nk, nh), i...  29.1 us
    ppermute x12, starting transfers between devices, take_from(): return lax.ppermute(a, axis, [((i + shift) % size, i) for i in range(size)])  21.5 us
    all_to_all x1, blocking collectives, shards(): lax.all_to_all(pairs, 'tp', split_axis=0, concat_axis=0, tiled=True)  13.8 us
    pallas_call x1, Pallas kernels, source_grad(): pl.pallas_call(source_kernel, grid=(steps,), in_specs=[pl.BlockSpec((head...  10.8 us
    ppermute x12, waiting for transfers between devices, take_from(): return lax.ppermute(a, axis, [((i + shift) % size, i) for i in range(size)])  10.3 us
  transfers between devices with their start and end apart: 27, of which 12 were waited for; matrix products, arithmetic and copies ran while one was open for 6% of the time, Pallas kernels for 34%

profile of v1, /device:TPU:0, one launch (start us, length us, event | category | flops | bytes accessed | tf_op | source)
XLA Modules:
  0.0 294.7 jit_solution(12940606786283114697)
XLA Ops:
  8.6 2.0 fusion.3
  10.7 34.7 %all-gather.5.cloned.1.call-done = bf16[512,4096]{1,0:T(8,128)(2,1)} async-done(((bf16[64,4096]{1,0:T(8,128)(2,1)}), bf16[512,4096]{1,0:T(8,128)(2,1)}) %all-gather.5.cloned.1.call-update) | async-done | bytes 4194320 | tf_op jit(solution)/shard_map/all_gather | solution.py:331
  45.4 7.3 %pairs.1 = bf16[8,128,128]{2,1,0:T(8,128)(2,1)} custom-call(bf16[128,4096]{1,0:T(8,128)(2,1)} %x_ref.5, f32[1,4096]{1,0:T(1,128)} %bitcast.241, bf16[4096,512]{1,0:T(8,128)(2,1)} %wk_ref.3, bf16[4096,512]{1,0:T(8,128)(2,1)} %wv_ref.3), custom_call_target="tpu_custom_call" | custom-call | tf_op jit(solution)/shard_map/pairs/pallas_call | solution.py:41
  52.7 13.8 %all_to_all.15 = bf16[8,128,128]{2,1,0:T(8,128)(2,1)S(1)} all-to-all(bf16[8,128,128]{2,1,0:T(8,128)(2,1)} %pairs.1), channel_id=1, replica_groups=mesh['z'=4,'x'=4,'tp'=8] {'tp'}, dimensions={0} | all-to-all | bytes 524288 | tf_op jit(solution)/shard_map/all_to_all | solution.py:333
  67.9 2.7 collective-permute-start.4
  72.1 3.8 %fusion = bf16[512,128]{0,1:T(8,128)(2,1)S(1)} fusion(bf16[512,4096]{1,0:T(8,128)(2,1)} %all-gather.5.cloned.1.call-done, bf16[4096,128]{1,0:T(8,128)(2,1)S(1)} %copy-done.2), kind=kOutput, calls=%fused_computation.5 | convolution fusion | flops 537001984 | bytes 5373952 | tf_op jit(solution)/shard_map/dot_general | solution.py:337
  77.5 2.9 collective-permute-start.1
  86.2 29.1 %forward.1 = (bf16[4,128,512]{2,1,0:T(8,128)(2,1)}, f32[4,2,8,512]{3,2,1,0:T(8,128)}, bf16[4,8,1024,512]{3,2,1,0:T(8,128)(2,1)}, bf16[4,128,1024]{2,1,0:T(8,128)(2,1)}) custom-call(bf16[4,128,512]{2,1,0:T(8,128)(2,1)} %pad_maximum_fusion.1.qt_ref, bf16[4,1024,128]{2,1,0:T(8,128)(2,1)} %pad_maximum_fusion.kv_ref), custom_call_target="tpu_custom_call" | custom-call | flops 40000000000 | bytes 40000000 | tf_op jit(solution)/shard_map/forward/pallas_call | solution.py:96
  116.4 3.9 %convolution_convert_fusion.1 = bf16[512,128]{0,1:T(8,128)(2,1)S(1)} fusion(bf16[512,4096]{1,0:T(8,128)(2,1)} %all-gather.7.cloned.1.call-done, bf16[128,4096]{1,0:T(8,128)(2,1)S(1)} %copy-done), kind=kOutput, calls=%fused_computation.4 | convolution fusion | flops 536936448 | bytes 5373952 | tf_op jit(solution)/shard_map/dot_general | solution.py:345
  121.5 3.0 %collective-permute-start.7 = (bf16[128,512]{1,0:T(8,128)(2,1)S(1)}, bf16[128,512]{1,0:T(8,128)(2,1)S(1)}, u32[]{:S(2)}, u32[]{:S(2)}) collective-permute-start(bf16[128,512]{1,0:T(8,128)(2,1)S(1)} %bitcast.223), channel_id=1, source_target_pairs={{64,0},{96,32},{0,64},{32,96},{65,1},{97,33},{1,65},{33,97},{66,2}... | collective-permute-start | bytes 393224 | tf_op jit(solution)/shard_map/ppermute | solution.py:310
  126.8 1.9 collective-permute-done.7
  130.9 2.1 collective-permute-start.20
  134.8 2.1 collective-permute-start.9
  138.9 3.6 %collective-permute-done.10 = f32[4,3,2,512]{3,2,0,1:T(2,128)S(1)} collective-permute-done((f32[4,3,2,512]{3,2,0,1:T(2,128)S(1)}, f32[4,3,2,512]{3,2,0,1:T(2,128)S(1)}, u32[]{:S(2)}, u32[]{:S(2)}) %collective-permute-start.10) | collective-permute-done | bytes 49184 | tf_op jit(solution)/shard_map/ppermute | solution.py:310
  148.2 39.3 %backward1.1 = (bf16[3,1024,128]{2,1,0:T(8,128)(2,1)}, f32[8,64,512]{2,1,0:T(8,128)}) custom-call(f32[4,2,8,512]{3,2,1,0:T(8,128)} %maximum_maximum_fusion.w_ref, bf16[4,128,512]{2,1,0:T(8,128)(2,1)} %pad_maximum_fusion.1.qt_ref, bf16[4,128,512]{2,1,0:T(8,128)(2,1)} %pad_maximum_fusion.2.dot_ref, bf16[4,1024,128]{2,1,0:T(8,128)(2,1)} %pad_maximum_fusion.kv_ref, ...), custom_call_target="tpu_custom_call" | custom-call | flops 51000000512 | bytes 27000000 | tf_op jit(solution)/shard_map/backward1/pallas_call | solution.py:187
  188.7 2.3 collective-permute-start.17
  192.0 14.5 %backward0.1 = (f32[1,1024,128]{2,1,0:T(8,128)}, f32[8,64,512]{2,1,0:T(8,128)}) custom-call(f32[4,2,8,512]{3,2,1,0:T(8,128)} %maximum_maximum_fusion.w_ref, bf16[4,128,512]{2,1,0:T(8,128)(2,1)} %pad_maximum_fusion.1.qt_ref, bf16[4,128,512]{2,1,0:T(8,128)(2,1)} %pad_maximum_fusion.2.dot_ref, bf16[4,1024,128]{2,1,0:T(8,128)(2,1)} %pad_maximum_fusion.kv_ref, ...), custom_call_target="tpu_custom_call" | custom-call | flops 16999999488 | bytes 9000000 | tf_op jit(solution)/shard_map/backward0/pallas_call | solution.py:187
  212.1 3.4 %all-to-all-start.2 = ((bf16[8,128,128]{2,1,0:T(8,128)(2,1)}), bf16[8,128,128]{2,1,0:T(8,128)(2,1)S(1)}, u32[]{:S(2)}, u32[]{:S(2)}) async-start(bf16[8,128,128]{2,1,0:T(8,128)(2,1)} %bitcast.46), calls=%async_computation.2 | async-start | bytes 524288 | tf_op jit(solution)/shard_map/all_to_all | solution.py:392
  217.5 5.5 %all-to-all-done.2.dkv_ref = bf16[8,128,128]{2,1,0:T(8,128)(2,1)S(1)} async-done(((bf16[8,128,128]{2,1,0:T(8,128)(2,1)}), bf16[8,128,128]{2,1,0:T(8,128)(2,1)S(1)}, u32[]{:S(2)}, u32[]{:S(2)}) %all-to-all-start.2) | async-done | bytes 262176 | tf_op jit(solution)/shard_map/all_to_all | solution.py:392
  223.0 3.4 %all-to-all-start.1 = ((bf16[8,64,128]{2,1,0:T(8,128)(2,1)}), bf16[8,64,128]{2,1,0:T(8,128)(2,1)S(1)}, u32[]{:S(2)}, u32[]{:S(2)}) async-start(bf16[8,64,128]{2,1,0:T(8,128)(2,1)} %bitcast.39), calls=%async_computation.1 | async-start | bytes 262144 | tf_op jit(solution)/shard_map/all_to_all | solution.py:397
  226.4 10.8 %source_grad.1 = f32[128,4096]{1,0:T(8,128)} custom-call(bf16[8,128,128]{2,1,0:T(8,128)(2,1)} %copy-done.5, bf16[4096,512]{1,0:T(8,128)(2,1)} %wk_ref.3, bf16[4096,512]{1,0:T(8,128)(2,1)} %wv_ref.3, bf16[128,4096]{1,0:T(8,128)(2,1)} %x_ref.5, f32[1,4096]{1,0:T(1,128)} %bitcast.242), custom_call_target="tpu_custom_call" | custom-call | tf_op jit(solution)/shard_map/source_grad/pallas_call | solution.py:252
  237.2 2.9 convert_element_type.115
  240.0 38.7 %all-gather.9.cloned.1.call-done = bf16[32768,128]{1,0:T(8,128)(2,1)} async-done(((bf16[4096,128]{1,0:T(8,128)(2,1)}), bf16[32768,128]{1,0:T(8,128)(2,1)}) %all-gather.9.cloned.1.call-update) | async-done | bytes 8388624 | tf_op jit(solution)/shard_map/all_gather | solution.py:349
  278.8 9.4 %target_grad.1 = f32[64,4096]{1,0:T(8,128)} custom-call(bf16[8,64,128]{2,1,0:T(8,128)(2,1)} %copy-done.6, bf16[8,4096,128]{2,1,0:T(8,128)(2,1)} %bitcast.209, bf16[64,4096]{1,0:T(8,128)(2,1)} %x_ref.4, f32[1,4096]{1,0:T(1,128)} %bitcast.243), custom_call_target="tpu_custom_call" | custom-call | tf_op jit(solution)/shard_map/target_grad/pallas_call | solution.py:293
  (107 shorter events, 37.6 us)
Async XLA Ops:
  7.2 38.2 %all-gather.5.cloned.1.call-start = ((), (), s32[]{:S(2)}) async-start(), calls=%async_computation.3 | async-start | bytes 4718592 | tf_op jit(solution)/shard_map/all_gather | solution.py:331
  10.6 105.8 %all-gather.7.cloned.1.call-start = ((), (), s32[]{:S(2)}) async-start(), calls=%async_computation.4 | async-start | bytes 4718592 | tf_op jit(solution)/shard_map/all_gather | solution.py:344
  45.4 191.8 %all-reduce.2.cloned.1.call-start = ((), (), s32[]{:S(2)}) async-start(), calls=%async_computation.5 | async-start | bytes 2097152 | tf_op jit(solution)/shard_map/psum | solution.py:380
  66.5 13.9 %collective-permute-start.5 = (bf16[1024,128]{1,0:T(8,128)(2,1)S(1)}, bf16[1024,128]{1,0:T(8,128)(2,1)S(1)}, u32[]{:S(2)}, u32[]{:S(2)}) collective-permute-start(bf16[1024,128]{1,0:T(8,128)(2,1)S(1)} %bitcast.211), channel_id=1, source_target_pairs={{24,0},{0,8},{8,16},{16,24},{25,1},{1,9},{9,17},{17,25},{26,2},{2,... | collective-permute-start | bytes 786440 | tf_op jit(solution)/shard_map/ppermute | solution.py:310
  67.9 13.8 %collective-permute-start.4 = (bf16[1024,128]{1,0:T(8,128)(2,1)S(1)}, bf16[1024,128]{1,0:T(8,128)(2,1)S(1)}, u32[]{:S(2)}, u32[]{:S(2)}) collective-permute-start(bf16[1024,128]{1,0:T(8,128)(2,1)S(1)} %bitcast.212), channel_id=1, source_target_pairs={{16,0},{24,8},{0,16},{8,24},{17,1},{25,9},{1,17},{9,25},{18,2},{26... | collective-permute-start | bytes 786440 | tf_op jit(solution)/shard_map/ppermute | solution.py:310
  70.6 11.1 %collective-permute-start.3 = (bf16[1024,128]{1,0:T(8,128)(2,1)S(1)}, bf16[1024,128]{1,0:T(8,128)(2,1)S(1)}, u32[]{:S(2)}, u32[]{:S(2)}) collective-permute-start(bf16[1024,128]{1,0:T(8,128)(2,1)S(1)} %bitcast.213), channel_id=1, source_target_pairs={{8,0},{16,8},{24,16},{0,24},{9,1},{17,9},{25,17},{1,25},{10,2},{18... | collective-permute-start | bytes 786440 | tf_op jit(solution)/shard_map/ppermute | solution.py:310
  75.9 7.7 %collective-permute-start.2 = (bf16[128,512]{1,0:T(8,128)(2,1)S(1)}, bf16[128,512]{1,0:T(8,128)(2,1)S(1)}, u32[]{:S(2)}, u32[]{:S(2)}) collective-permute-start(bf16[128,512]{1,0:T(8,128)(2,1)S(1)} %bitcast.215), channel_id=1, source_target_pairs={{96,0},{0,32},{32,64},{64,96},{97,1},{1,33},{33,65},{65,97},{98,2}... | collective-permute-start | bytes 393224 | tf_op jit(solution)/shard_map/ppermute | solution.py:310
  77.5 7.6 %collective-permute-start.1 = (bf16[128,512]{1,0:T(8,128)(2,1)S(1)}, bf16[128,512]{1,0:T(8,128)(2,1)S(1)}, u32[]{:S(2)}, u32[]{:S(2)}) collective-permute-start(bf16[128,512]{1,0:T(8,128)(2,1)S(1)} %bitcast.216), channel_id=1, source_target_pairs={{64,0},{96,32},{0,64},{32,96},{65,1},{97,33},{1,65},{33,97},{66,2}... | collective-permute-start | bytes 393224 | tf_op jit(solution)/shard_map/ppermute | solution.py:310
  120.3 6.5 %collective-permute-start.8 = (bf16[128,512]{1,0:T(8,128)(2,1)S(1)}, bf16[128,512]{1,0:T(8,128)(2,1)S(1)}, u32[]{:S(2)}, u32[]{:S(2)}) collective-permute-start(bf16[128,512]{1,0:T(8,128)(2,1)S(1)} %bitcast.222), channel_id=1, source_target_pairs={{96,0},{0,32},{32,64},{64,96},{97,1},{1,33},{33,65},{65,97},{98,2}... | collective-permute-start | bytes 393224 | tf_op jit(solution)/shard_map/ppermute | solution.py:310
  121.5 7.3 %collective-permute-start.7 = (bf16[128,512]{1,0:T(8,128)(2,1)S(1)}, bf16[128,512]{1,0:T(8,128)(2,1)S(1)}, u32[]{:S(2)}, u32[]{:S(2)}) collective-permute-start(bf16[128,512]{1,0:T(8,128)(2,1)S(1)} %bitcast.223), channel_id=1, source_target_pairs={{64,0},{96,32},{0,64},{32,96},{65,1},{97,33},{1,65},{33,97},{66,2}... | collective-permute-start | bytes 393224 | tf_op jit(solution)/shard_map/ppermute | solution.py:310
  129.6 7.3 %collective-permute-start.11 = (f32[4,3,2,512]{3,2,0,1:T(2,128)S(1)}, f32[4,3,2,512]{3,2,0,1:T(2,128)S(1)}, u32[]{:S(2)}, u32[]{:S(2)}) collective-permute-start(f32[4,3,2,512]{3,2,0,1:T(2,128)S(1)} %pad_maximum_fusion.3), channel_id=1, source_target_pairs={{96,0},{0,32},{32,64},{64,96},{97,1},{1,33},{33,65},{65,97},{98,2}... | collective-permute-start | bytes 147464 | tf_op jit(solution)/shard_map/ppermute | solution.py:310
  130.9 11.8 %collective-permute-start.20 = (bf16[128,512]{1,0:T(8,128)(2,1)S(1)}, bf16[128,512]{1,0:T(8,128)(2,1)S(1)}, u32[]{:S(2)}, u32[]{:S(2)}) collective-permute-start(bf16[128,512]{1,0:T(8,128)(2,1)S(1)} %get-tuple-element.39), channel_id=1, source_target_pairs={{0,96},{32,0},{64,32},{96,64},{1,97},{33,1},{65,33},{97,65},{2,98}... | collective-permute-start | bytes 393224 | tf_op jit(solution)/shard_map/ppermute | solution.py:314
  133.0 9.6 %collective-permute-start.19 = (bf16[128,512]{1,0:T(8,128)(2,1)S(1)}, bf16[128,512]{1,0:T(8,128)(2,1)S(1)}, u32[]{:S(2)}, u32[]{:S(2)}) collective-permute-start(bf16[128,512]{1,0:T(8,128)(2,1)S(1)} %get-tuple-element.40), channel_id=1, source_target_pairs={{0,64},{32,96},{64,0},{96,32},{1,65},{33,97},{65,1},{97,33},{2,66}... | collective-permute-start | bytes 393224 | tf_op jit(solution)/shard_map/ppermute | solution.py:314
  133.6 9.0 %collective-permute-start.18 = (bf16[128,512]{1,0:T(8,128)(2,1)S(1)}, bf16[128,512]{1,0:T(8,128)(2,1)S(1)}, u32[]{:S(2)}, u32[]{:S(2)}) collective-permute-start(bf16[128,512]{1,0:T(8,128)(2,1)S(1)} %get-tuple-element.38), channel_id=1, source_target_pairs={{0,32},{32,64},{64,96},{96,0},{1,33},{33,65},{65,97},{97,1},{2,34}... | collective-permute-start | bytes 393224 | tf_op jit(solution)/shard_map/ppermute | solution.py:314
  136.9 5.6 %collective-permute-start.10 = (f32[4,3,2,512]{3,2,0,1:T(2,128)S(1)}, f32[4,3,2,512]{3,2,0,1:T(2,128)S(1)}, u32[]{:S(2)}, u32[]{:S(2)}) collective-permute-start(f32[4,3,2,512]{3,2,0,1:T(2,128)S(1)} %pad_maximum_fusion.3), channel_id=1, source_target_pairs={{64,0},{96,32},{0,64},{32,96},{65,1},{97,33},{1,65},{33,97},{66,2}... | collective-permute-start | bytes 147464 | tf_op jit(solution)/shard_map/ppermute | solution.py:310
  144.5 134.2 %all-gather.9.cloned.1.call-start = ((), (), s32[]{:S(2)}) async-start(), calls=%async_computation.6 | async-start | bytes 9437184 | tf_op jit(solution)/shard_map/all_gather | solution.py:349
  188.7 21.4 %collective-permute-start.17 = (bf16[1024,128]{1,0:T(8,128)(2,1)S(1)}, bf16[1024,128]{1,0:T(8,128)(2,1)S(1)}, u32[]{:S(2)}, u32[]{:S(2)}) collective-permute-start(bf16[1024,128]{1,0:T(8,128)(2,1)S(1)} %get-tuple-element.36), channel_id=1, source_target_pairs={{0,24},{8,0},{16,8},{24,16},{1,25},{9,1},{17,9},{25,17},{2,26},{10... | collective-permute-start | bytes 786440 | tf_op jit(solution)/shard_map/ppermute | solution.py:314
  191.0 20.3 %collective-permute-start.16 = (bf16[1024,128]{1,0:T(8,128)(2,1)S(1)}, bf16[1024,128]{1,0:T(8,128)(2,1)S(1)}, u32[]{:S(2)}, u32[]{:S(2)}) collective-permute-start(bf16[1024,128]{1,0:T(8,128)(2,1)S(1)} %get-tuple-element.37), channel_id=1, source_target_pairs={{0,16},{8,24},{16,0},{24,8},{1,17},{9,25},{17,1},{25,9},{2,18},{10... | collective-permute-start | bytes 786440 | tf_op jit(solution)/shard_map/ppermute | solution.py:314
  191.7 19.7 %collective-permute-start.15 = (bf16[1024,128]{1,0:T(8,128)(2,1)S(1)}, bf16[1024,128]{1,0:T(8,128)(2,1)S(1)}, u32[]{:S(2)}, u32[]{:S(2)}) collective-permute-start(bf16[1024,128]{1,0:T(8,128)(2,1)S(1)} %get-tuple-element.35), channel_id=1, source_target_pairs={{0,8},{8,16},{16,24},{24,0},{1,9},{9,17},{17,25},{25,1},{2,10},{10... | collective-permute-start | bytes 786440 | tf_op jit(solution)/shard_map/ppermute | solution.py:314
  208.3 7.3 %collective-permute-start.14 = (bf16[128,512]{0,1:T(8,128)(2,1)S(1)}, bf16[128,512]{0,1:T(8,128)(2,1)S(1)}, u32[]{:S(2)}, u32[]{:S(2)}) collective-permute-start(bf16[128,512]{0,1:T(8,128)(2,1)S(1)} %copy.43), channel_id=1, source_target_pairs={{0,96},{32,0},{64,32},{96,64},{1,97},{33,1},{65,33},{97,65},{2,98}... | collective-permute-start | bytes 393224 | tf_op jit(solution)/shard_map/ppermute | solution.py:314
  208.8 6.8 %collective-permute-start.13 = (bf16[128,512]{0,1:T(8,128)(2,1)S(1)}, bf16[128,512]{0,1:T(8,128)(2,1)S(1)}, u32[]{:S(2)}, u32[]{:S(2)}) collective-permute-start(bf16[128,512]{0,1:T(8,128)(2,1)S(1)} %copy.42), channel_id=1, source_target_pairs={{0,64},{32,96},{64,0},{96,32},{1,65},{33,97},{65,1},{97,33},{2,66}... | collective-permute-start | bytes 393224 | tf_op jit(solution)/shard_map/ppermute | solution.py:314
  210.1 6.7 %collective-permute-start.12 = (bf16[128,512]{0,1:T(8,128)(2,1)S(1)}, bf16[128,512]{0,1:T(8,128)(2,1)S(1)}, u32[]{:S(2)}, u32[]{:S(2)}) collective-permute-start(bf16[128,512]{0,1:T(8,128)(2,1)S(1)} %copy.41), channel_id=1, source_target_pairs={{0,32},{32,64},{64,96},{96,0},{1,33},{33,65},{65,97},{97,1},{2,34}... | collective-permute-start | bytes 393224 | tf_op jit(solution)/shard_map/ppermute | solution.py:314
  212.1 10.9 %all-to-all-start.2 = ((bf16[8,128,128]{2,1,0:T(8,128)(2,1)}), bf16[8,128,128]{2,1,0:T(8,128)(2,1)S(1)}, u32[]{:S(2)}, u32[]{:S(2)}) async-start(bf16[8,128,128]{2,1,0:T(8,128)(2,1)} %bitcast.46), calls=%async_computation.2 | async-start | bytes 524288 | tf_op jit(solution)/shard_map/all_to_all | solution.py:392
  223.0 17.0 %all-to-all-start.1 = ((bf16[8,64,128]{2,1,0:T(8,128)(2,1)}), bf16[8,64,128]{2,1,0:T(8,128)(2,1)S(1)}, u32[]{:S(2)}, u32[]{:S(2)}) async-start(bf16[8,64,128]{2,1,0:T(8,128)(2,1)} %bitcast.39), calls=%async_computation.1 | async-start | bytes 262144 | tf_op jit(solution)/shard_map/all_to_all | solution.py:397
  (12 other events, 250.3 us)
Sparse Core Ops, SparseCore 0:
  10.7 34.5 all-gather.4
  47.0 34.6 all-gather.6
  144.6 83.7 all-reduce.1
  230.0 48.7 all-gather.8
